TPU v7x, 256 devices: a whole 4x4x8 slice. The times are simulated.
256 devices in a mesh: sp: 16 (over y, x), tp: 16 (over z, core).
Axes of the slice: x: 4, y: 4, z: 8, core: 2. Of those that a mesh axis runs over, the one named last changes fastest.
Arguments:
- queries: bfloat16 [32768, 2048], P('sp', 'tp'), may hold values from -160 to 160
- key_heads: bfloat16 [32768, 512], P('sp'), may hold values from -8 to 8
- value_heads: bfloat16 [32768, 512], P('sp'), may hold values from -4 to 4
- sink_logit: float32 [16], P('tp'), may hold values from -2 to 7
- out_weight: bfloat16 [2048, 2048], P('tp'), may hold values from -0.125 to 0.125
- residual: bfloat16 [32768, 2048], P(('sp', 'tp')), may hold values from -6 to 6
- mixer_gain: float32 [2048], replicated, may hold values from 0.1 to 1.9
- expert_gain: float32 [2048], replicated, may hold values from 0.1 to 1.9
- route_group: int32 [32768], P(('sp', 'tp')), may hold values from 0 to 15, as said below
- route_member: int32 [32768, 2], P(('sp', 'tp')), may hold values from 0 to 2, as said below
- route_weight: bfloat16 [32768, 2], P(('sp', 'tp')), may hold values from 0.19921875 to 1
- gate_weight: bfloat16 [48, 2048, 2048], P('sp', None, 'tp'), may hold values from -0.125 to 0.125
- up_weight: bfloat16 [48, 2048, 2048], P('sp', None, 'tp'), may hold values from -0.125 to 0.125
- down_weight: bfloat16 [48, 2048, 2048], P('sp', 'tp'), may hold values from -0.125 to 0.125
Outputs:
- output: bfloat16 [32768, 2048], P(('sp', 'tp'))
Inputs may be any that keep to these rules, and one draw needn't show every extreme that they name: `route_group`: among the tokens of one device, at most 10 name one group; in every draw one group is named by exactly 10 tokens of every device. `route_member`: the two entries of a token are different members of its group.
All inputs are finite; a program needn't handle non-finite values.
Results may differ from a plain program's by a relative error of at most 0.018.
Values may be sent and summed in bfloat16 or wider, within the bound.
A program may use at most 128 MiB of HBM per device.

v0:
```python
import jax
import jax.numpy as jnp
from jax import lax
from jax.sharding import Mesh
from jax.sharding import PartitionSpec as P

HEADS = 16
KV_HEADS = 4
HEAD_DIM = 128
WINDOW = 128
BLOCK = 128
GROUP_EXPERTS = 3
TP = ("tp_0", "tp_1")
SP_TP = ("sp", "tp_0", "tp_1")
EPS = 1e-06
NEG_BIG = -1e30


def extended(block, sides, width):
    for axis, dim in sides:
        count = lax.axis_size(axis)
        forward = [(i, i + 1) for i in range(count - 1)]
        backward = [(target, source) for source, target in forward]
        low = lax.ppermute(
            lax.slice_in_dim(block, block.shape[dim] - width, None, axis=dim), axis, forward
        )
        high = lax.ppermute(lax.slice_in_dim(block, 0, width, axis=dim), axis, backward)
        block = jnp.concatenate([low, block, high], axis=dim)
    return block


def cut_along(shard, dim, devices):
    dims = shard.shape
    blocks = shard.reshape(*dims[:dim], devices, dims[dim] // devices, *dims[dim + 1 :])
    return jnp.moveaxis(blocks, dim, 0)


def joined_along(blocks, dim):
    dims = list(blocks.shape[1:])
    dims[dim] *= blocks.shape[0]
    return jnp.moveaxis(blocks, 0, dim).reshape(dims)


def exchange_in_order(blocks, axes, order):
    dims = [lax.axis_size(a) for a in axes]
    blocks = blocks.reshape(*dims, *blocks.shape[1:])
    for k in order:
        blocks = lax.all_to_all(blocks, axes[k], split_axis=k, concat_axis=k, tiled=True)
    return blocks.reshape(-1, *blocks.shape[len(axes) :])


def stepwise_exchange(shard, axes, order, split_dim, concat_dim):
    blocks = cut_along(shard, split_dim, lax.axis_size(axes))
    return joined_along(exchange_in_order(blocks, axes, order), concat_dim)


def window_attention(queries, key_heads, value_heads, sink_logit):
    seq_rows = queries.shape[0]
    heads_dev = sink_logit.shape[0]
    key_group = HEADS // KV_HEADS
    key_start = lax.axis_index(TP) * heads_dev // key_group * HEAD_DIM
    key_own = lax.dynamic_slice_in_dim(key_heads, key_start, HEAD_DIM, 1)
    value_own = lax.dynamic_slice_in_dim(value_heads, key_start, HEAD_DIM, 1)
    padded = extended(jnp.stack([key_own, value_own]), (("sp", 1),), WINDOW)
    blocks = seq_rows // BLOCK
    extent = WINDOW // BLOCK
    tile_rows = padded.reshape(2, blocks + 2 * extent, BLOCK, HEAD_DIM)
    key_spans = jnp.concatenate(
        [tile_rows[:, shifted : shifted + blocks] for shifted in range(2 * extent + 1)], axis=2
    )
    offset = lax.axis_index("sp") * seq_rows
    seq_total = seq_rows * lax.axis_size("sp")
    query_pos = offset + jnp.arange(seq_rows, dtype=jnp.int32).reshape(blocks, BLOCK)
    key_pos = (
        offset
        + (jnp.arange(blocks, dtype=jnp.int32) * BLOCK)[:, None]
        + jnp.arange(BLOCK + 2 * WINDOW, dtype=jnp.int32)[None, :]
        - WINDOW
    )
    inside = (
        (jnp.abs(query_pos[:, :, None] - key_pos[:, None, :]) <= WINDOW)
        & (key_pos >= 0)[:, None, :]
        & (key_pos < seq_total)[:, None, :]
    )
    query_blocks = queries.reshape(blocks, BLOCK, heads_dev, HEAD_DIM)
    scores = jnp.einsum(
        "nqhd,nkd->nhqk", query_blocks, key_spans[0], preferred_element_type=jnp.float32
    ) * HEAD_DIM ** (-0.5)
    scores = jnp.where(inside[:, None], scores, NEG_BIG)
    sink_col = sink_logit[None, :, None, None]
    row_top = jnp.maximum(jnp.max(scores, axis=3, keepdims=True), sink_col)
    exp_terms = jnp.exp(scores - row_top)
    row_mass = jnp.sum(exp_terms, axis=3, keepdims=True) + jnp.exp(sink_col - row_top)
    weight = (exp_terms / row_mass).astype(jnp.bfloat16)
    attended = jnp.einsum(
        "nhqk,nkd->nqhd", weight, key_spans[1], preferred_element_type=jnp.float32
    ).astype(jnp.bfloat16)
    return attended.reshape(seq_rows, heads_dev * HEAD_DIM)


def per_device(
    queries,
    key_heads,
    value_heads,
    sink_logit,
    out_weight,
    residual,
    mixer_gain,
    expert_gain,
    route_group,
    route_member,
    route_weight,
    gate_weight,
    up_weight,
    down_weight,
):
    attended = window_attention(queries, key_heads, value_heads, sink_logit)
    tok_rows = residual.shape[0]
    width = out_weight.shape[1]
    by_token = stepwise_exchange(attended, TP, (1, 0), 0, 1)
    shard_rows = out_weight.shape[0]
    weight_piece = lax.all_gather(out_weight, TP, axis=0, tiled=True)
    shards = weight_piece.shape[0] // shard_rows
    columns = by_token
    columns = columns.reshape(tok_rows, shards, shard_rows)
    weight_slabs = weight_piece.reshape(shards, shard_rows, width)
    products = jnp.einsum("rkc,kcd->krd", columns, weight_slabs, preferred_element_type=jnp.float32)
    rounded = lax.optimization_barrier(products.astype(jnp.bfloat16))
    projected = jnp.sum(rounded.astype(jnp.float32), axis=0)
    proj_scale = lax.rsqrt(jnp.mean(projected * projected, axis=1, keepdims=True) + EPS)
    mixed_rows = (residual.astype(jnp.float32) + mixer_gain * (projected * proj_scale)).astype(
        jnp.bfloat16
    )
    mixed_float = mixed_rows.astype(jnp.float32)
    norm_scale = lax.rsqrt(jnp.mean(mixed_float * mixed_float, axis=1, keepdims=True) + EPS)
    normed = (mixed_float * norm_scale * expert_gain).astype(jnp.bfloat16)
    groups = lax.axis_size("sp")
    capacity = max(2, (5 * tok_rows + 4 * groups - 1) // (4 * groups))
    group_ids = jnp.arange(groups, dtype=jnp.int32)
    chosen = (route_group[:, None] == group_ids[None, :]).astype(jnp.int32)
    group_rank = jnp.sum(chosen * (jnp.cumsum(chosen, axis=0) - 1), axis=1)
    slot_ids = route_group * capacity + group_rank
    placing = (jnp.arange(groups * capacity, dtype=jnp.int32)[:, None] == slot_ids[None, :]).astype(
        jnp.bfloat16
    )
    member_ids = jnp.arange(GROUP_EXPERTS, dtype=jnp.int32)
    token_gates = jnp.sum(
        route_weight.astype(jnp.float32)[:, :, None]
        * (route_member[:, :, None] == member_ids[None, None, :]).astype(jnp.float32),
        axis=1,
    ).astype(jnp.bfloat16)
    send_rows = (
        jnp.dot(placing, normed, preferred_element_type=jnp.float32)
        .astype(jnp.bfloat16)
        .reshape(groups, capacity, width)
    )
    send_gates = (
        jnp.dot(placing, token_gates, preferred_element_type=jnp.float32)
        .astype(jnp.bfloat16)
        .reshape(groups, capacity, GROUP_EXPERTS)
    )
    arrived_rows, arrived_gates = (
        lax.all_to_all(send_rows, "sp", split_axis=0, concat_axis=0, tiled=True),
        lax.all_to_all(send_gates, "sp", split_axis=0, concat_axis=0, tiled=True),
    )
    pooled_rows, pooled_gates = (
        lax.all_gather(arrived_rows, TP, axis=0, tiled=True),
        lax.all_gather(arrived_gates, TP, axis=0, tiled=True),
    )
    flat_rows = pooled_rows.reshape(-1, width)
    flat_gates = pooled_gates.reshape(-1, GROUP_EXPERTS).astype(jnp.float32)
    gate_pre = jnp.einsum("md,edh->meh", flat_rows, gate_weight, preferred_element_type=jnp.float32)
    up_pre = jnp.einsum("md,edh->meh", flat_rows, up_weight, preferred_element_type=jnp.float32)
    hidden = (jax.nn.silu(gate_pre) * up_pre * flat_gates[:, :, None]).astype(jnp.bfloat16)
    partial_out = jnp.einsum("meh,ehd->md", hidden, down_weight, preferred_element_type=jnp.float32)
    summed = lax.psum_scatter(
        partial_out.reshape(pooled_rows.shape).astype(jnp.bfloat16),
        TP,
        scatter_dimension=0,
        tiled=True,
    )
    returned = lax.all_to_all(summed, "sp", split_axis=0, concat_axis=0, tiled=True)
    expert_out = lax.dot_general(
        placing,
        returned.reshape(groups * capacity, width),
        (((0,), (0,)), ((), ())),
        preferred_element_type=jnp.float32,
    )
    return (mixed_float + expert_out).astype(jnp.bfloat16)


def solution(mesh):
    torus = Mesh(mesh.devices.reshape(mesh.shape["sp"], 8, 2), ("sp", "tp_0", "tp_1"))
    placed = (
        P("sp", TP),
        P("sp", None),
        P("sp", None),
        P(TP),
        P(TP, None),
        P(SP_TP, None),
        P(),
        P(),
        P(SP_TP),
        P(SP_TP, None),
        P(SP_TP, None),
        P("sp", None, TP),
        P("sp", None, TP),
        P("sp", TP, None),
    )
    return jax.shard_map(
        per_device, mesh=torus, in_specs=placed, out_specs=P(SP_TP, None), check_vma=False
    )
```

profile of v0, /device:TPU:33, one launch (start us, length us, event | category | flops | bytes accessed | tf_op | source)
XLA Modules:
  0.0 387.4 jit_solution(15848808001674454527)
XLA Ops:
  6.5 0.7 all-gather.3.cloned.1.call-update
  7.3 1.3 dynamic-slice_bitcast_fusion
  8.6 3.1 collective-permute-start
  11.7 1.3 collective-permute-start.1
  13.7 0.1 fusion.22
  13.9 2.9 collective-permute-done.1
  16.7 0.1 pad_maximum_fusion.1
  16.8 0.8 fusion.25
  17.6 0.4 pad_maximum_fusion
  18.0 0.6 copy-done.6
  18.6 4.1 %fusion.26 = (f32[16,128]{1,0:T(8,128)S(1)}, f32[16,1,128,384]{2,3,0,1:T(8,128)S(1)}) fusion(bf16[16,128,128]{2,1,0:T(8,128)(2,1)S(1)} %bitcast.66, bf16[2,16,384,128]{3,2,1,0:T(8,128)(2,1)S(1)} %pad_maximum_fusion, pred[16,384]{1,0:T(8,128)(4,1)S(1)} %get-tuple-element.13, pred[16,384]{1,0:T(8,128)(4,1)S(1)} %get-tuple-element.12, ...), kind=kOutput, calls=%fused_computation.58 | convolution fusion | flops 207616000 | bytes 5296128 | tf_op jit(solution)/shard_map/nqhd,nkd->nhqk/dot_general | solution.py:86
  22.8 0.4 fusion.4
  23.2 1.0 fusion.8
  24.3 5.9 %all_to_all.25 = bf16[8,2,128,128]{2,3,0,1:T(8,128)(2,1)S(1)} all-to-all(bf16[8,2,128,128]{2,3,0,1:T(8,128)(2,1)S(1)} %copy.57), channel_id=1, replica_groups=mesh['sp'=16,'tp_0'=8,'tp_1'=2] {'tp_1'}, dimensions={1} | all-to-all | bytes 1048576 | tf_op jit(solution)/shard_map/all_to_all | solution.py:48
  30.2 0.8 copy.58
  31.1 8.0 %all-to-all-start.1 = ((bf16[8,2,128,128]{2,3,1,0:T(8,128)(2,1)}), bf16[8,2,128,128]{2,3,1,0:T(8,128)(2,1)S(1)}, u32[]{:S(2)}, u32[]{:S(2)}) async-start(bf16[8,2,128,128]{2,3,1,0:T(8,128)(2,1)} %copy.58), calls=%async_computation.1 | async-start | bytes 1048576 | tf_op jit(solution)/shard_map/all_to_all | solution.py:48
  39.1 0.1 fusion.17
  39.2 0.2 reduce_window_sum.11
  39.3 0.2 select_reduce_fusion
  39.5 21.6 %all-to-all-done.1 = bf16[8,2,128,128]{2,3,1,0:T(8,128)(2,1)S(1)} async-done(((bf16[8,2,128,128]{2,3,1,0:T(8,128)(2,1)}), bf16[8,2,128,128]{2,3,1,0:T(8,128)(2,1)S(1)}, u32[]{:S(2)}, u32[]{:S(2)}) %all-to-all-start.1) | async-done | bytes 524320 | tf_op jit(solution)/shard_map/all_to_all | solution.py:48
  61.1 0.3 copy.59
  61.4 16.1 %all-gather.3.cloned.1.call-done = bf16[2048,2048]{1,0:T(8,128)(2,1)} async-done(((bf16[128,2048]{1,0:T(8,128)(2,1)}), bf16[2048,2048]{1,0:T(8,128)(2,1)}) %all-gather.3.cloned.1.call-update) | async-done | bytes 8388624 | tf_op jit(solution)/shard_map/all_gather | solution.py:122
  77.5 5.7 %convolution_convert_fusion = bf16[16,128,2048]{2,1,0:T(8,128)(2,1)S(1)} fusion(bf16[128,16,128]{2,0,1:T(8,128)(2,1)S(1)} %bitcast.64, bf16[16,128,2048]{2,1,0:T(8,128)(2,1)} %bitcast.62), kind=kOutput, calls=%fused_computation.2 | convolution fusion | flops 1077936128 | bytes 17301504 | tf_op jit(solution)/shard_map/rkc,kcd->krd/dot_general | solution.py:127
  83.3 1.8 convert_reduce_fusion
  85.1 0.2 multiply_reduce_fusion
  85.3 0.4 fusion.11
  85.7 0.1 copy-done.3
  85.8 1.3 convolution_convert_fusion.1
  87.1 1.3 reshape.189
  88.4 22.7 %all_to_all.26 = bf16[16,10,2048]{2,1,0:T(8,128)(2,1)S(1)} all-to-all(bf16[16,10,2048]{2,1,0:T(8,128)(2,1)S(1)} %reshape.189), channel_id=1, replica_groups=mesh['sp'=16,'tp_0'=8,'tp_1'=2] {'sp'}, dimensions={0} | all-to-all | bytes 1310720 | tf_op jit(solution)/shard_map/all_to_all | solution.py:163
  111.1 1.2 copy.60
  112.5 0.1 convolution_convert_fusion.2
  112.6 0.1 reshape.191
  112.8 9.6 %all_to_all.27 = bf16[16,10,3]{1,2,0:T(4,128)(2,1)S(1)} all-to-all(bf16[16,10,3]{1,2,0:T(4,128)(2,1)S(1)} %copy.62), channel_id=1, replica_groups=mesh['sp'=16,'tp_0'=8,'tp_1'=2] {'sp'}, dimensions={0} | all-to-all | bytes 1920 | tf_op jit(solution)/shard_map/all_to_all | solution.py:164
  122.3 21.6 %all_gather.11 = bf16[256,10,3]{1,2,0:T(4,128)(2,1)S(1)} all-gather(bf16[16,10,3]{1,2,0:T(4,128)(2,1)S(1)} %all_to_all.27), channel_id=1, replica_groups=mesh['sp'=16,'tp_0'=8,'tp_1'=2] {'tp_0','tp_1'}, dimensions={0}, use_global_device_ids=true | all-gather | bytes 16320 | tf_op jit(solution)/shard_map/all_gather | solution.py:168
  144.0 0.2 copy.63
  144.1 0.2 copy.64
  144.3 0.3 reshape.193
  144.6 30.9 %all-gather.5.cloned.1.call-done = bf16[256,10,2048]{2,0,1:T(8,128)(2,1)} async-done(((bf16[16,10,2048]{2,0,1:T(8,128)(2,1)}), bf16[256,10,2048]{2,0,1:T(8,128)(2,1)}) %all-gather.5.cloned.1.call-update) | async-done | bytes 10485776 | tf_op jit(solution)/shard_map/all_gather | solution.py:167
  175.5 15.4 %copy.61 = bf16[256,10,2048]{2,1,0:T(8,128)(2,1)} copy(bf16[256,10,2048]{2,0,1:T(8,128)(2,1)} %all-gather.5.cloned.1.call-done) | data formatting | bytes 20971520 | tf_op jit(solution)/shard_map/all_gather | solution.py:167
  190.9 18.1 %reshape.194 = bf16[2560,2048,1]{1,0,2:T(8,128)(2,1)} reshape(bf16[256,10,2048]{2,1,0:T(8,128)(2,1)} %copy.61) | data formatting | bytes 20971520 | tf_op jit(solution)/shard_map/reshape | solution.py:170
  209.0 10.0 %fusion.27 = f32[2560,3,128]{2,0,1:T(8,128)} fusion(bf16[2560,2048,1]{1,0,2:T(8,128)(2,1)} %reshape.194, bf16[3,2048,128]{2,1,0:T(8,128)(2,1)} %param.25), kind=kOutput, calls=%fused_computation.59 | convolution fusion | flops 4026531840 | bytes 15990784 | tf_op jit(solution)/shard_map/md,edh->meh/dot_general | solution.py:172
  219.0 16.4 %bitcast_convert_fusion = bf16[2560,2048]{1,0:T(8,128)(2,1)} fusion(bf16[3,128,2048]{2,1,0:T(8,128)(2,1)S(1)} %copy-done, bf16[2560,2048,1]{1,0,2:T(8,128)(2,1)} %reshape.194, bf16[3,2048,128]{2,1,0:T(8,128)(2,1)} %param.26, f32[2560,3,128]{2,0,1:T(8,128)} %fusion.27, f32[2560,3]{0,1:T(4,128)S(1)} %reshape.193), kind=kOutput, calls=%fused_computation | convolution fusion | flops 8065187840 | bytes 28080128 | tf_op jit(solution)/shard_map/meh,ehd->md/dot_general | solution.py:175
  235.4 17.7 %convert_element_type.88 = bf16[256,10,2048]{2,1,0:T(8,128)(2,1)} reshape(bf16[2560,2048]{1,0:T(8,128)(2,1)} %bitcast_convert_fusion) | data formatting | bytes 20971520 | tf_op jit(solution)/shard_map/convert_element_type | solution.py:177
  253.1 99.7 %reduce-scatter.2.cloned.1.call-done = bf16[16,10,2048]{2,1,0:T(8,128)(2,1)} async-done(((bf16[256,10,2048]{2,1,0:T(8,128)(2,1)}), bf16[16,10,2048]{2,1,0:T(8,128)(2,1)}) %reduce-scatter.2.cloned.1.call-update) | async-done | bytes 655376 | tf_op jit(solution)/shard_map/reduce_scatter | solution.py:176
  352.8 24.8 %all_to_all.28 = bf16[16,10,2048]{2,1,0:T(8,128)(2,1)S(1)} all-to-all(bf16[16,10,2048]{2,1,0:T(8,128)(2,1)} %reduce-scatter.2.cloned.1.call-done), channel_id=1, replica_groups=mesh['sp'=16,'tp_0'=8,'tp_1'=2] {'sp'}, dimensions={0} | all-to-all | bytes 1310720 | tf_op jit(solution)/shard_map/all_to_all | solution.py:182
  377.6 1.1 reshape.192
  378.7 2.2 fusion.5
  (33 shorter events, 0.3 us)
Async XLA Ops:
  6.5 212.5 %copy-start = (bf16[3,128,2048]{2,1,0:T(8,128)(2,1)S(1)}, bf16[3,128,2048]{2,1,0:T(8,128)(2,1)}, u32[]{:S(2)}) copy-start(bf16[3,128,2048]{2,1,0:T(8,128)(2,1)} %param.27) | copy-start | bytes 4718596
  6.5 71.0 %all-gather.3.cloned.1.call-start = ((), (), s32[]{:S(2)}) async-start(), calls=%async_computation.6 | async-start | bytes 8912896 | tf_op jit(solution)/shard_map/all_gather | solution.py:122
  8.6 5.3 %collective-permute-start = (bf16[2,128,128]{2,1,0:T(8,128)(2,1)S(1)}, bf16[2,128,128]{2,1,0:T(8,128)(2,1)S(1)}, u32[]{:S(2)}, u32[]{:S(2)}) collective-permute-start(bf16[2,128,128]{2,1,0:T(8,128)(2,1)S(1)} %get-tuple-element.10), channel_id=1, source_target_pairs={{0,16},{16,32},{32,48},{48,64},{64,80},{80,96},{96,112},{112,128},... | collective-permute-start | bytes 196616 | tf_op jit(solution)/shard_map/ppermute | solution.py:24
  11.7 5.0 %collective-permute-start.1 = (bf16[2,128,128]{2,1,0:T(8,128)(2,1)S(1)}, bf16[2,128,128]{2,1,0:T(8,128)(2,1)S(1)}, u32[]{:S(2)}, u32[]{:S(2)}) collective-permute-start(bf16[2,128,128]{2,1,0:T(8,128)(2,1)S(1)} %get-tuple-element.11), channel_id=1, source_target_pairs={{16,0},{32,16},{48,32},{64,48},{80,64},{96,80},{112,96},{128,112},... | collective-permute-start | bytes 196616 | tf_op jit(solution)/shard_map/ppermute | solution.py:27
  17.6 1.0 copy-start.6
  24.3 14.8 %copy-start.4 = (s32[128]{0:T(128)S(1)}, s32[128]{0:T(128)}, u32[]{:S(2)}) copy-start(s32[128]{0:T(128)} %param.22) | copy-start | bytes 1540
  31.1 30.1 %all-to-all-start.1 = ((bf16[8,2,128,128]{2,3,1,0:T(8,128)(2,1)}), bf16[8,2,128,128]{2,3,1,0:T(8,128)(2,1)S(1)}, u32[]{:S(2)}, u32[]{:S(2)}) async-start(bf16[8,2,128,128]{2,3,1,0:T(8,128)(2,1)} %copy.58), calls=%async_computation.1 | async-start | bytes 1048576 | tf_op jit(solution)/shard_map/all_to_all | solution.py:48
  39.1 136.5 %all-gather.5.cloned.1.call-start = ((), (), s32[]{:S(2)}) async-start(), calls=%async_computation.7 | async-start | bytes 11141120 | tf_op jit(solution)/shard_map/all_gather | solution.py:167
  83.2 2.1 copy-start.1
  83.2 2.0 copy-start.2
  85.1 0.7 copy-start.3
  87.1 25.4 %copy-start.7 = (bf16[128,2]{0,1:T(2,128)(2,1)S(1)}, bf16[128,2]{0,1:T(2,128)(2,1)}, u32[]{:S(2)}) copy-start(bf16[128,2]{0,1:T(2,128)(2,1)} %param.24) | copy-start | bytes 1540
  87.1 25.4 %copy-start.5 = (s32[128,2]{0,1:T(2,128)S(1)}, s32[128,2]{0,1:T(2,128)}, u32[]{:S(2)}) copy-start(s32[128,2]{0,1:T(2,128)} %param.23) | copy-start | bytes 3076
  112.4 240.4 %reduce-scatter.2.cloned.1.call-start = ((), (), s32[]{:S(2)}) async-start(), calls=%async_computation.8 | async-start | bytes 17825792 | tf_op jit(solution)/shard_map/reduce_scatter | solution.py:176
Sparse Core Ops, SparseCore 0:
  9.2 68.3 all-gather.2
  112.5 62.9 all-gather.4
  253.2 99.5 reduce-scatter.1
where the time goes:
time: 389 us; the launch traced here: 387 us
  waiting for transfers between devices  172 us (44%)
  blocking collectives  84.6 us (22%)
  local copies, waits for them, and re-layouts  59.5 us (15%)
  matrix products  40.9 us (11%)
  between operations  14 us (4%)
  starting transfers between devices  12.5 us (3%)
  other arithmetic  3.92 us (1%)
    reduce_scatter x1, waiting for transfers between devices, per_device(): lax.psum_scatter(partial_out.reshape(pooled_rows.shape).astype(jnp.bfloat...  99.7 us
    all_gather x1, waiting for transfers between devices, per_device(): lax.all_gather(arrived_rows, TP, axis=0, tiled=True)  30.9 us
    all_to_all x1, blocking collectives, per_device(): lax.all_to_all(summed, 'sp', split_axis=0, concat_axis=0, tiled=True)  24.8 us
    all_to_all x1, blocking collectives, per_device(): lax.all_to_all(send_rows, 'sp', split_axis=0, concat_axis=0, tiled=True)  22.7 us
    all_gather x1, blocking collectives, per_device(): lax.all_gather(arrived_gates, TP, axis=0, tiled=True)  21.6 us
    all_to_all x1, waiting for transfers between devices, exchange_in_order(): lax.all_to_all(blocks, axes[k], split_axis=k, concat_axis=k, tiled=True)  21.6 us
    reshape x1, local copies, waits for them, and re-layouts, per_device(): flat_rows = pooled_rows.reshape(-1, width)  18.1 us
    convert_element_type x1, local copies, waits for them, and re-layouts, per_device(): partial_out.reshape(pooled_rows.shape).astype(jnp.bfloat16)  17.7 us
  transfers between devices with their start and end apart: 6, of which 5 were waited for; matrix products, arithmetic and copies ran while one was open for 3% of the time, Pallas kernels for 0%

commit v1 on v0

--- a/solution.py
+++ b/solution.py
@@ -164,7 +164,9 @@
         lax.all_to_all(send_gates, "sp", split_axis=0, concat_axis=0, tiled=True),
     )
     pooled_rows, pooled_gates = (
-        lax.all_gather(arrived_rows, TP, axis=0, tiled=True),
+        jnp.concatenate(
+            lax.all_to_all(jnp.stack([arrived_rows] * lax.axis_size(TP)), TP, 0, 0), axis=0
+        ),
         lax.all_gather(arrived_gates, TP, axis=0, tiled=True),
     )
     flat_rows = pooled_rows.reshape(-1, width)

time: 389 us -> 587 us (1.51)
  blocking collectives: 84.6 us -> 270 us
  starting transfers between devices: 12.5 us -> 32 us
  waiting for transfers between devices: 172 us -> 158 us
  local copies, waits for them, and re-layouts: 59.5 us -> 66.3 us
    all_gather x1, blocking collectives: 21.6 us -> 239 us  [per_device(): lax.all_gather(arrived_gates, TP, axis=0, tiled=True)]
    all_to_all x2 -> x0, blocking collectives: 32.3 us -> none  [the longest x1 22.7 us: per_device(): lax.all_to_all(send_rows, 'sp', split_axis=0, concat_axis=0, tiled=True)]
    all_gather x1 -> x0, waiting for transfers between devices: 30.9 us -> none  [per_device(): lax.all_gather(arrived_rows, TP, axis=0, tiled=True)]
    another operation x0 -> x2, local copies, waits for them, and re-layouts: none -> 24.5 us  [the longest x1 18.1 us: per_device(): flat_rows = pooled_rows.reshape(-1, width)]
    all_to_all x0 -> x3, waiting for transfers between devices: none -> 20.7 us  [the longest x1 15.5 us: per_device(): lax.all_to_all(send_rows, 'sp', split_axis=0, concat_axis=0, tiled=True)]
    all_to_all x0 -> x3, starting transfers between devices: none -> 19.6 us  [the longest x1 8.57 us: per_device(): lax.all_to_all(jnp.stack([arrived_rows] * lax.axis_size(TP)), TP, 0, 0)]
    reshape x1 -> x0, local copies, waits for them, and re-layouts: 18.1 us -> none  [per_device(): flat_rows = pooled_rows.reshape(-1, width)]
    all_gather x1 -> x0, local copies, waits for them, and re-layouts: 15.4 us -> none  [per_device(): lax.all_gather(arrived_rows, TP, axis=0, tiled=True)]
  transfers between devices with their start and end apart: 6 -> 8, of which waited for: 5 -> 6; matrix products, arithmetic and copies ran while one was open for 3% -> 2% of each run, Pallas kernels for 0% -> 0%
where the time goes in v1:
time: 587 us; the launch traced here: 585 us
  blocking collectives  270 us (46%)
  waiting for transfers between devices  158 us (27%)
  local copies, waits for them, and re-layouts  66.3 us (11%)
  matrix products  40 us (7%)
  starting transfers between devices  32 us (5%)
  between operations  14.4 us (2%)
    all_gather x1, blocking collectives, per_device(): lax.all_gather(arrived_gates, TP, axis=0, tiled=True)  239 us
    reduce_scatter x1, waiting for transfers between devices, per_device(): lax.psum_scatter(partial_out.reshape(pooled_rows.shape).astype(jnp.bfloat...  96.2 us
    all_to_all x1, blocking collectives, per_device(): lax.all_to_all(summed, 'sp', split_axis=0, concat_axis=0, tiled=True)  24.8 us
    all_to_all x1, waiting for transfers between devices, exchange_in_order(): lax.all_to_all(blocks, axes[k], split_axis=k, concat_axis=k, tiled=True)  21.6 us
    another operation x1, local copies, waits for them, and re-layouts, per_device(): flat_rows = pooled_rows.reshape(-1, width)  18.1 us
    convert_element_type x1, local copies, waits for them, and re-layouts, per_device(): partial_out.reshape(pooled_rows.shape).astype(jnp.bfloat16)  17.7 us
    dot_general x1, matrix products, per_device(): jnp.einsum('meh,ehd->md', hidden, down_weight, preferred_element_type=jnp...  16.4 us
    all_gather x1, waiting for transfers between devices, per_device(): weight_piece = lax.all_gather(out_weight, TP, axis=0, tiled=True)  16.1 us
  transfers between devices with their start and end apart: 8, of which 6 were waited for; matrix products, arithmetic and copies ran while one was open for 2% of the time, Pallas kernels for 0%

profile of v1, /device:TPU:33, one launch (start us, length us, event | category | flops | bytes accessed | tf_op | source)
XLA Modules:
  0.0 584.6 jit_solution(15012397416453293349)
XLA Ops:
  6.5 0.7 all-gather.2.cloned.1.call-update
  7.3 1.3 dynamic-slice_bitcast_fusion
  8.6 3.1 collective-permute-start
  11.7 1.3 collective-permute-start.1
  13.9 2.9 collective-permute-done.1
  16.8 0.8 fusion.25
  17.6 0.4 pad_maximum_fusion
  18.0 0.6 copy-done.6
  18.6 4.1 fusion.26
  22.8 0.4 fusion.4
  23.2 1.0 fusion.8
  24.3 5.9 %all_to_all.30 = bf16[8,2,128,128]{2,3,0,1:T(8,128)(2,1)S(1)} all-to-all(bf16[8,2,128,128]{2,3,0,1:T(8,128)(2,1)S(1)} %copy.57), channel_id=1, replica_groups=mesh['sp'=16,'tp_0'=8,'tp_1'=2] {'tp_1'}, dimensions={1} | all-to-all | bytes 1048576 | tf_op jit(solution)/shard_map/all_to_all | solution.py:48
  30.2 0.8 copy.58
  31.1 8.0 %all-to-all-start.1 = ((bf16[8,2,128,128]{2,3,1,0:T(8,128)(2,1)}), bf16[8,2,128,128]{2,3,1,0:T(8,128)(2,1)S(1)}, u32[]{:S(2)}, u32[]{:S(2)}) async-start(bf16[8,2,128,128]{2,3,1,0:T(8,128)(2,1)} %copy.58), calls=%async_computation.1 | async-start | bytes 1048576 | tf_op jit(solution)/shard_map/all_to_all | solution.py:48
  39.1 0.2 reduce_window_sum.11
  39.3 0.2 select_reduce_fusion
  39.5 21.6 %all-to-all-done.1 = bf16[8,2,128,128]{2,3,1,0:T(8,128)(2,1)S(1)} async-done(((bf16[8,2,128,128]{2,3,1,0:T(8,128)(2,1)}), bf16[8,2,128,128]{2,3,1,0:T(8,128)(2,1)S(1)}, u32[]{:S(2)}, u32[]{:S(2)}) %all-to-all-start.1) | async-done | bytes 524320 | tf_op jit(solution)/shard_map/all_to_all | solution.py:48
  61.1 0.3 copy.59
  61.4 16.1 %all-gather.2.cloned.1.call-done = bf16[2048,2048]{1,0:T(8,128)(2,1)} async-done(((bf16[128,2048]{1,0:T(8,128)(2,1)}), bf16[2048,2048]{1,0:T(8,128)(2,1)}) %all-gather.2.cloned.1.call-update) | async-done | bytes 8388624 | tf_op jit(solution)/shard_map/all_gather | solution.py:122
  77.5 5.7 convolution_convert_fusion
  83.3 1.8 convert_reduce_fusion
  85.1 0.2 multiply_reduce_fusion
  85.3 0.4 fusion.11
  85.8 0.4 convolution_convert_fusion.1
  86.2 1.2 reshape.188
  87.4 6.5 %all-to-all-start.2 = ((bf16[16,10,2048]{2,1,0:T(8,128)(2,1)}), bf16[16,10,2048]{2,1,0:T(8,128)(2,1)S(1)}, u32[]{:S(2)}, u32[]{:S(2)}) async-start(bf16[16,10,2048]{2,1,0:T(8,128)(2,1)} %reshape.188), calls=%async_computation.2 | async-start | bytes 2097152 | tf_op jit(solution)/shard_map/all_to_all | solution.py:163
  94.0 0.1 convolution_convert_fusion.2
  94.1 0.1 reshape.189
  94.2 0.6 copy.62
  94.8 15.5 %all-to-all-done.2 = bf16[16,10,2048]{2,1,0:T(8,128)(2,1)S(1)} async-done(((bf16[16,10,2048]{2,1,0:T(8,128)(2,1)}), bf16[16,10,2048]{2,1,0:T(8,128)(2,1)S(1)}, u32[]{:S(2)}, u32[]{:S(2)}) %all-to-all-start.2) | async-done | bytes 655392 | tf_op jit(solution)/shard_map/all_to_all | solution.py:163
  110.3 4.5 all-to-all-start.4
  114.9 1.2 copy.60
  116.1 5.2 all-to-all-done.4
  121.3 6.4 %stack.11 = bf16[16,16,10,2048]{3,1,2,0:T(8,128)(2,1)} broadcast(bf16[16,10,2048]{2,0,1:T(8,128)(2,1)} %copy.60), dimensions={1,2,3} | broadcast | bytes 11141120 | tf_op jit(solution)/shard_map/stack | solution.py:168
  127.7 8.6 %all-to-all-start.3 = ((bf16[16,16,10,2048]{3,1,2,0:T(8,128)(2,1)}), bf16[16,16,10,2048]{3,1,2,0:T(8,128)(2,1)}, u32[]{:S(2)}, u32[]{:S(2)}) async-start(bf16[16,16,10,2048]{3,1,2,0:T(8,128)(2,1)} %stack.11), calls=%async_computation.3 | async-start | bytes 20971520 | tf_op jit(solution)/shard_map/all_to_all | solution.py:168
  136.3 239.0 %all_gather.7 = bf16[256,10,3]{1,2,0:T(4,128)(2,1)S(1)} all-gather(bf16[16,10,3]{1,2,0:T(4,128)(2,1)S(1)} %all-to-all-done.4), channel_id=1, replica_groups=mesh['sp'=16,'tp_0'=8,'tp_1'=2] {'tp_0','tp_1'}, dimensions={0}, use_global_device_ids=true | all-gather | bytes 16320 | tf_op jit(solution)/shard_map/all_gather | solution.py:170
  375.3 0.2 copy.63
  375.5 0.2 copy.64
  375.7 0.3 reshape.191
  375.9 15.4 %copy.61 = bf16[16,16,10,2048]{3,2,1,0:T(8,128)(2,1)} copy(bf16[16,16,10,2048]{3,1,2,0:T(8,128)(2,1)} %all-to-all-done.3) | data formatting | bytes 20971520 | tf_op jit(solution)/shard_map/all_to_all | solution.py:168
  391.3 18.1 %reshape.192 = bf16[2560,2048,1]{1,0,2:T(8,128)(2,1)} reshape(bf16[16,16,10,2048]{3,2,1,0:T(8,128)(2,1)} %copy.61) | data formatting | bytes 20971520 | tf_op jit(solution)/shard_map/reshape;reshape | solution.py:172
  409.4 10.0 %fusion.27 = f32[2560,3,128]{2,0,1:T(8,128)} fusion(bf16[2560,2048,1]{1,0,2:T(8,128)(2,1)} %reshape.192, bf16[3,2048,128]{2,1,0:T(8,128)(2,1)} %param.25), kind=kOutput, calls=%fused_computation.59 | convolution fusion | flops 4026531840 | bytes 15990784 | tf_op jit(solution)/shard_map/md,edh->meh/dot_general | solution.py:174
  419.4 16.4 %bitcast_convert_fusion = bf16[2560,2048]{1,0:T(8,128)(2,1)} fusion(bf16[3,128,2048]{2,1,0:T(8,128)(2,1)S(1)} %copy-done, bf16[2560,2048,1]{1,0,2:T(8,128)(2,1)} %reshape.192, bf16[3,2048,128]{2,1,0:T(8,128)(2,1)} %param.26, f32[2560,3,128]{2,0,1:T(8,128)} %fusion.27, f32[2560,3]{0,1:T(4,128)S(1)} %reshape.191), kind=kOutput, calls=%fused_computation | convolution fusion | flops 8065187840 | bytes 28080128 | tf_op jit(solution)/shard_map/meh,ehd->md/dot_general | solution.py:177
  435.8 17.7 %convert_element_type.88 = bf16[256,10,2048]{2,1,0:T(8,128)(2,1)} reshape(bf16[2560,2048]{1,0:T(8,128)(2,1)} %bitcast_convert_fusion) | data formatting | bytes 20971520 | tf_op jit(solution)/shard_map/convert_element_type | solution.py:179
  453.5 96.2 %reduce-scatter.2.cloned.1.call-done = bf16[16,10,2048]{2,1,0:T(8,128)(2,1)} async-done(((bf16[256,10,2048]{2,1,0:T(8,128)(2,1)}), bf16[16,10,2048]{2,1,0:T(8,128)(2,1)}) %reduce-scatter.2.cloned.1.call-update) | async-done | bytes 655376 | tf_op jit(solution)/shard_map/reduce_scatter | solution.py:178
  549.7 24.8 %all_to_all.31 = bf16[16,10,2048]{2,1,0:T(8,128)(2,1)S(1)} all-to-all(bf16[16,10,2048]{2,1,0:T(8,128)(2,1)} %reduce-scatter.2.cloned.1.call-done), channel_id=1, replica_groups=mesh['sp'=16,'tp_0'=8,'tp_1'=2] {'sp'}, dimensions={0} | all-to-all | bytes 1310720 | tf_op jit(solution)/shard_map/all_to_all | solution.py:184
  574.5 1.1 reshape.190
  575.5 2.2 fusion.5
  (35 shorter events, 0.6 us)
Async XLA Ops:
  6.5 412.8 %copy-start = (bf16[3,128,2048]{2,1,0:T(8,128)(2,1)S(1)}, bf16[3,128,2048]{2,1,0:T(8,128)(2,1)}, u32[]{:S(2)}) copy-start(bf16[3,128,2048]{2,1,0:T(8,128)(2,1)} %param.27) | copy-start | bytes 4718596
  6.5 71.0 %all-gather.2.cloned.1.call-start = ((), (), s32[]{:S(2)}) async-start(), calls=%async_computation.7 | async-start | bytes 8912896 | tf_op jit(solution)/shard_map/all_gather | solution.py:122
  8.6 5.3 collective-permute-start
  11.7 5.0 collective-permute-start.1
  17.6 1.0 copy-start.6
  24.3 14.8 %copy-start.4 = (s32[128]{0:T(128)S(1)}, s32[128]{0:T(128)}, u32[]{:S(2)}) copy-start(s32[128]{0:T(128)} %param.22) | copy-start | bytes 1540
  31.1 30.1 %all-to-all-start.1 = ((bf16[8,2,128,128]{2,3,1,0:T(8,128)(2,1)}), bf16[8,2,128,128]{2,3,1,0:T(8,128)(2,1)S(1)}, u32[]{:S(2)}, u32[]{:S(2)}) async-start(bf16[8,2,128,128]{2,3,1,0:T(8,128)(2,1)} %copy.58), calls=%async_computation.1 | async-start | bytes 1048576 | tf_op jit(solution)/shard_map/all_to_all | solution.py:48
  83.2 2.1 copy-start.1
  83.2 2.0 copy-start.2
  85.1 0.7 copy-start.3
  85.3 8.6 %copy-start.7 = (bf16[128,2]{0,1:T(2,128)(2,1)S(1)}, bf16[128,2]{0,1:T(2,128)(2,1)}, u32[]{:S(2)}) copy-start(bf16[128,2]{0,1:T(2,128)(2,1)} %param.24) | copy-start | bytes 1540
  85.3 8.6 %copy-start.5 = (s32[128,2]{0,1:T(2,128)S(1)}, s32[128,2]{0,1:T(2,128)}, u32[]{:S(2)}) copy-start(s32[128,2]{0,1:T(2,128)} %param.23) | copy-start | bytes 3076
  87.4 22.9 %all-to-all-start.2 = ((bf16[16,10,2048]{2,1,0:T(8,128)(2,1)}), bf16[16,10,2048]{2,1,0:T(8,128)(2,1)S(1)}, u32[]{:S(2)}, u32[]{:S(2)}) async-start(bf16[16,10,2048]{2,1,0:T(8,128)(2,1)} %reshape.188), calls=%async_computation.2 | async-start | bytes 2097152 | tf_op jit(solution)/shard_map/all_to_all | solution.py:163
  110.3 10.9 %all-to-all-start.4 = ((bf16[16,10,3]{1,2,0:T(4,128)(2,1)}), bf16[16,10,3]{1,2,0:T(4,128)(2,1)S(1)}, u32[]{:S(2)}, u32[]{:S(2)}) async-start(bf16[16,10,3]{1,2,0:T(4,128)(2,1)} %copy.62), calls=%async_computation.4 | async-start | bytes 32768 | tf_op jit(solution)/shard_map/all_to_all | solution.py:164
  127.7 248.2 %all-to-all-start.3 = ((bf16[16,16,10,2048]{3,1,2,0:T(8,128)(2,1)}), bf16[16,16,10,2048]{3,1,2,0:T(8,128)(2,1)}, u32[]{:S(2)}, u32[]{:S(2)}) async-start(bf16[16,16,10,2048]{3,1,2,0:T(8,128)(2,1)} %stack.11), calls=%async_computation.3 | async-start | bytes 20971520 | tf_op jit(solution)/shard_map/all_to_all | solution.py:168
  136.3 413.4 %reduce-scatter.2.cloned.1.call-start = ((), (), s32[]{:S(2)}) async-start(), calls=%async_computation.8 | async-start | bytes 17825792 | tf_op jit(solution)/shard_map/reduce_scatter | solution.py:178
Sparse Core Ops, SparseCore 0:
  9.2 68.3 all-gather.1
  453.6 96.0 reduce-scatter.1
